TPU v7x, 32 devices: a whole 2x2x4 slice. The times are simulated.
32 devices in a mesh: sp: 8 (over z, x), tp: 4 (over y, core).
Axes of the slice: x: 2, y: 2, z: 4, core: 2. Of those that a mesh axis runs over, the one named last changes fastest.
Arguments:
- hidden_rows: bfloat16 [1024, 2048], P('sp', 'tp'), may hold values from -6 to 6
- out_cot: bfloat16 [1024, 2048], P('sp', 'tp'), may hold values from -6 to 6
- routes: int32 [1024, 2], P('sp'), may hold values from 0 to 7, all different within a row; in each aligned block of 128 rows (0 to 127, 128 to 255, ...) at most 40 rows name the same one
- route_weight: float32 [1024, 2], P('sp'), may hold values from 0.2 to 2
- gate_w: bfloat16 [8, 2048, 1024], P('sp', None, 'tp'), may hold values from -0.125 to 0.125
- up_w: bfloat16 [8, 2048, 1024], P('sp', None, 'tp'), may hold values from -0.125 to 0.125
- down_w: bfloat16 [8, 1024, 2048], P('sp', 'tp'), may hold values from -0.1875 to 0.1875
- out_weight: bfloat16 [2048, 4096], P('sp', 'tp'), may hold values from -0.09375 to 0.09375
- step_inputs: bfloat16 [1024, 4096], P('sp', 'tp'), may hold values from -6 to 6
- input_map: bfloat16 [1024, 1024], P('sp', 'tp'), may hold values from -2 to 2
- output_map: bfloat16 [1024, 1024], P('sp', 'tp'), may hold values from -2 to 2
- log_decay: float32 [1024, 64], P('sp', 'tp'), may hold values from -1 to 0, as said below
- gate_z: bfloat16 [1024, 4096], P('sp', 'tp'), may hold values from -6 to 6
Outputs:
- grad_gate_w: float32 [8, 2048, 1024], P('sp', None, 'tp')
- grad_up_w: float32 [8, 2048, 1024], P('sp', None, 'tp')
- grad_down_w: float32 [8, 1024, 2048], P('sp', 'tp')
- grad_out_weight: float32 [2048, 4096], P('sp', 'tp')
- grad_step: bfloat16 [1024, 4096], P('sp', 'tp')
- grad_gate_z: bfloat16 [1024, 4096], P('sp', 'tp')
- grad_input_map: float32 [1024, 1024], P('sp', 'tp')
- grad_output_map: float32 [1024, 1024], P('sp', 'tp')
- grad_log_decay: float32 [1024, 64], P('sp', 'tp')
Inputs may be any that keep to these rules, and one draw needn't show every extreme that they name: `routes`: each row names 2 different experts. Among the positions of one index of sp no expert is named more than 40 times, a bound that some block reaches. `log_decay`: every entry is negative.
All inputs are finite; a program needn't handle non-finite values.
Results may differ from a plain program's by a relative error of at most 0.015.
Values may be sent and summed in bfloat16 or wider, within the bound.
A program may use at most 128 MiB of HBM per device.

v0:
```python
from functools import reduce

import jax
import jax.numpy as jnp
from jax import lax
from jax.sharding import PartitionSpec as P

D = 2048
HEAD_DIM = 64
NS = 128
BLOCK = 128


epsilon = 1e-06
exact_mode = lax.Precision.HIGHEST
by_rows = (((0,), (0,)), ((), ()))
by_cols = (((1,), (1,)), ((), ()))


def entering(part, axis, combine, identity, reverse):
    count = lax.axis_size(axis)
    place = lax.axis_index(axis)
    ahead = count - 1 - place if reverse else place
    gathered = jax.tree.map(lambda a: lax.all_gather(a, axis), part)
    state = jax.tree.map(lambda a, e: jnp.zeros_like(a) + jnp.asarray(e, a.dtype), part, identity)

    def one(hop, state):
        source = count - 1 - hop if reverse else hop
        return combine(
            state, jax.tree.map(lambda a: lax.dynamic_index_in_dim(a, source, 0, False), gathered)
        )

    return lax.fori_loop(0, ahead, one, state)


def block_step(carry_state, inputs):
    x_block, b_block, c_block, log_block = inputs
    per_group = x_block.shape[1] // b_block.shape[1]
    cum_log = jnp.cumsum(log_block, axis=0)
    token_places = jnp.arange(log_block.shape[0])
    lower_mask = (token_places[:, None] >= token_places[None, :])[:, :, None]
    log_spans = jnp.where(lower_mask, cum_log[:, None, :] - cum_log[None, :, :], 0.0)
    decay_mask = jnp.where(lower_mask, jnp.exp(log_spans), 0.0)
    scores = jnp.einsum("tgn,sgn->tsg", c_block, b_block, precision=exact_mode)
    scores = jnp.repeat(scores, per_group, axis=2)
    within = jnp.einsum("tsh,shp->thp", scores * decay_mask, x_block, precision=exact_mode)
    c_heads = jnp.repeat(c_block, per_group, axis=1)
    b_heads = jnp.repeat(b_block, per_group, axis=1)
    carried = (
        jnp.einsum("thn,hpn->thp", c_heads, carry_state, precision=exact_mode)
        * jnp.exp(cum_log)[:, :, None]
    )
    last_log = cum_log[-1]
    to_end = jnp.exp(last_log[None, :] - cum_log)
    new_state = carry_state * jnp.exp(last_log)[:, None, None] + jnp.einsum(
        "shn,shp->hpn", b_heads * to_end[:, :, None], x_block, precision=exact_mode
    )
    return (new_state, within + carried)


def mixer_forward(step_in, map_in, map_out, log_in, gate_in, entry_state):
    length, head_count = log_in.shape
    groups = map_in.shape[1] // NS
    blocks = length // BLOCK
    x_blocks = step_in.reshape(blocks, BLOCK, head_count, HEAD_DIM)
    b_blocks = map_in.reshape(blocks, BLOCK, groups, NS)
    c_blocks = map_out.reshape(blocks, BLOCK, groups, NS)
    log_blocks = log_in.reshape(blocks, BLOCK, head_count)
    _, outputs = lax.scan(block_step, entry_state, (x_blocks, b_blocks, c_blocks, log_blocks))
    mixed = outputs.reshape(length, head_count * HEAD_DIM)
    gated = (mixed * jax.nn.silu(gate_in)).reshape(length, groups, -1)
    normed = gated * lax.rsqrt(jnp.mean(gated * gated, axis=-1, keepdims=True) + epsilon)
    return normed.reshape(length, head_count * HEAD_DIM)


def segment_state(step_in, map_in, log_in):
    length, head_count = log_in.shape
    groups = map_in.shape[1] // NS
    cum_log = jnp.cumsum(log_in, axis=0)
    to_end = jnp.exp(cum_log[-1][None, :] - cum_log)
    b_heads = jnp.repeat(map_in.reshape(length, groups, NS), head_count // groups, axis=1)
    own_state = jnp.einsum(
        "shn,shp->hpn",
        b_heads * to_end[:, :, None],
        step_in.reshape(length, head_count, HEAD_DIM),
        precision=exact_mode,
    )
    return (jnp.exp(cum_log[-1]), own_state)


def compose_steps(earlier, later):
    return (earlier[0] * later[0], earlier[1] * later[0][:, None, None] + later[1])


def expert_backward(row_block, cot_block, gate_mat, up_mat, down_mat):
    gate_pre = jnp.dot(row_block, gate_mat, preferred_element_type=jnp.float32)
    up_pre = jnp.dot(row_block, up_mat, preferred_element_type=jnp.float32)
    gate_sigmoid = jax.nn.sigmoid(gate_pre)
    hidden = (gate_pre * gate_sigmoid * up_pre).astype(jnp.bfloat16)
    d_act = lax.dot_general(cot_block, down_mat, by_cols, preferred_element_type=jnp.float32)
    d_gate = (d_act * up_pre * gate_sigmoid * (1.0 + gate_pre * (1.0 - gate_sigmoid))).astype(
        jnp.bfloat16
    )
    d_up = (d_act * gate_pre * gate_sigmoid).astype(jnp.bfloat16)
    grad_down = lax.dot_general(hidden, cot_block, by_rows, preferred_element_type=jnp.float32)
    grad_gate = lax.dot_general(row_block, d_gate, by_rows, preferred_element_type=jnp.float32)
    grad_up = lax.dot_general(row_block, d_up, by_rows, preferred_element_type=jnp.float32)
    input_part = lax.dot_general(d_gate, gate_mat, by_cols, preferred_element_type=jnp.float32)
    input_part = input_part + lax.dot_general(
        d_up, up_mat, by_cols, preferred_element_type=jnp.float32
    )
    return (grad_gate, grad_up, grad_down, input_part)


def local(
    hidden_rows,
    out_cot,
    routes,
    route_weight,
    gate_w,
    up_w,
    down_w,
    out_weight,
    step_inputs,
    input_map,
    output_map,
    log_decay,
    gate_z,
):
    tok_rows, top_count = routes.shape
    local_experts = gate_w.shape[0]
    sp_devices = lax.axis_size("sp")
    total_experts = local_experts * sp_devices
    capacity = 5 * tok_rows * top_count // (4 * total_experts)
    flat_routes = routes.reshape(-1)
    expert_hits = (
        flat_routes[:, None] == jnp.arange(total_experts, dtype=jnp.int32)[None, :]
    ).astype(jnp.int32)
    slot_rank = jnp.sum((jnp.cumsum(expert_hits, axis=0) - expert_hits) * expert_hits, axis=1)
    target = (flat_routes * capacity + slot_rank).reshape(tok_rows, top_count)
    slot_ids = jnp.arange(total_experts * capacity, dtype=jnp.int32)[:, None]
    matches = [slot_ids == target[:, column][None, :] for column in range(top_count)]
    placing = reduce(jnp.logical_or, matches).astype(jnp.bfloat16)
    slot_weight = reduce(
        jnp.add,
        [
            jnp.sum(jnp.where(matches[column], route_weight[:, column][None, :], 0.0), axis=1)
            for column in range(top_count)
        ],
    )

    def place(source_rows):
        return jnp.dot(placing, source_rows, preferred_element_type=jnp.float32)

    sent_rows = place(hidden_rows).astype(jnp.bfloat16)
    sent_cot = (place(out_cot) * slot_weight[:, None]).astype(jnp.bfloat16)
    part_rows, part_cot = (
        lax.all_to_all(sent_rows, "sp", split_axis=0, concat_axis=0, tiled=True),
        lax.all_to_all(sent_cot, "sp", split_axis=0, concat_axis=0, tiled=True),
    )
    got_rows, got_cot = (
        lax.all_gather(part_rows, "tp", axis=1, tiled=True),
        lax.all_gather(part_cot, "tp", axis=1, tiled=True),
    )
    buffer_rows = sp_devices * capacity
    arranged_rows = (
        got_rows.reshape(sp_devices, local_experts, capacity, D)
        .transpose(1, 0, 2, 3)
        .reshape(local_experts, buffer_rows, D)
    )
    arranged_cot = (
        got_cot.reshape(sp_devices, local_experts, capacity, D)
        .transpose(1, 0, 2, 3)
        .reshape(local_experts, buffer_rows, D)
    )
    grad_gate, grad_up, grad_down, input_part = expert_backward(
        arranged_rows[0], arranged_cot[0], gate_w[0], up_w[0], down_w[0]
    )
    grads_gate = [grad_gate]
    grads_up = [grad_up]
    grads_down = [grad_down]
    partials = [input_part]
    stacked = (
        jnp.stack(partials)
        .reshape(local_experts, sp_devices, capacity, D)
        .transpose(1, 0, 2, 3)
        .reshape(-1, D)
    )
    summed = lax.psum_scatter(stacked.astype(jnp.bfloat16), "tp", scatter_dimension=1, tiled=True)
    returned = lax.all_to_all(summed, "sp", split_axis=0, concat_axis=0, tiled=True)
    routed = lax.dot_general(placing, returned, by_rows, preferred_element_type=jnp.float32)
    mid_part = (out_cot.astype(jnp.float32) + routed).astype(jnp.bfloat16)
    mid_grad = lax.all_gather(mid_part, "tp", axis=1, tiled=True)
    step_float = step_inputs.astype(jnp.float32)
    inmap_float = input_map.astype(jnp.float32)
    outmap_float = output_map.astype(jnp.float32)
    gates_float = gate_z.astype(jnp.float32)
    (decay_total, own_state), state_pullback = jax.vjp(
        segment_state, step_float, inmap_float, log_decay
    )
    identity = (jnp.ones_like(decay_total), jnp.zeros_like(own_state))
    _, entry_state = entering((decay_total, own_state), "sp", compose_steps, identity, False)
    normed, out_pullback = jax.vjp(
        mixer_forward, step_float, inmap_float, outmap_float, log_decay, gates_float, entry_state
    )
    normed_half = normed.astype(jnp.bfloat16)
    columns = mid_grad
    grad_out_weight = lax.psum_scatter(
        lax.dot_general(columns, normed_half, by_rows, preferred_element_type=jnp.float32),
        "sp",
        scatter_dimension=0,
        tiled=True,
    )
    columns = mid_grad
    d_normed = jnp.dot(
        columns,
        lax.all_gather(out_weight, "sp", axis=0, tiled=True),
        preferred_element_type=jnp.float32,
    )
    grad_step, grad_in_map, grad_out_map, grad_log, grad_gate, grad_entry = out_pullback(d_normed)
    _, carried_grad = entering((decay_total, grad_entry), "sp", compose_steps, identity, True)
    extra_step, extra_in_map, extra_log = state_pullback(
        (jnp.sum(carried_grad * entry_state, axis=(1, 2)), carried_grad)
    )
    return (
        jnp.stack(grads_gate),
        jnp.stack(grads_up),
        jnp.stack(grads_down),
        grad_out_weight,
        (grad_step + extra_step).astype(jnp.bfloat16),
        grad_gate.astype(jnp.bfloat16),
        grad_in_map + extra_in_map,
        grad_out_map,
        grad_log + extra_log,
    )


def solution(mesh):
    placed = (
        P("sp", "tp"),
        P("sp", "tp"),
        P("sp", None),
        P("sp", None),
        P("sp", None, "tp"),
        P("sp", None, "tp"),
        P("sp", "tp", None),
        P("sp", "tp"),
        P("sp", "tp"),
        P("sp", "tp"),
        P("sp", "tp"),
        P("sp", "tp"),
        P("sp", "tp"),
    )
    return jax.shard_map(
        local,
        mesh=mesh,
        in_specs=placed,
        out_specs=(
            P("sp", None, "tp"),
            P("sp", None, "tp"),
            P("sp", "tp", None),
            P("sp", "tp"),
            P("sp", "tp"),
            P("sp", "tp"),
            P("sp", "tp"),
            P("sp", "tp"),
            P("sp", "tp"),
        ),
        check_vma=False,
    )
```

profile of v0, /device:TPU:0, one launch (start us, length us, event | category | flops | bytes accessed | tf_op | source)
XLA Modules:
  0.0 479.5 jit_solution(6448955937463369872)
XLA Ops:
  12.3 18.1 %all_to_all.36 = bf16[8,40,512]{2,1,0:T(8,128)(2,1)} all-to-all(bf16[8,40,512]{2,1,0:T(8,128)(2,1)S(1)} %bitcast.223), channel_id=1, replica_groups=mesh['sp'=8,'tp'=4] {'sp'}, dimensions={0} | all-to-all | bytes 655360 | tf_op jit(solution)/shard_map/all_to_all | solution.py:158
  30.9 13.7 %all_to_all.37 = bf16[8,40,512]{2,1,0:T(8,128)(2,1)} all-to-all(bf16[8,40,512]{2,1,0:T(8,128)(2,1)S(1)} %bitcast.222), channel_id=1, replica_groups=mesh['sp'=8,'tp'=4] {'sp'}, dimensions={0} | all-to-all | bytes 655360 | tf_op jit(solution)/shard_map/all_to_all | solution.py:159
  44.7 2.4 all-gather.9.cloned.1.call-done
  47.2 1.9 fusion.15
  49.6 17.3 %all-gather.11.cloned.1.call-done = bf16[320,2048]{1,0:T(8,128)(2,1)} async-done(((bf16[320,512]{1,0:T(8,128)(2,1)}), bf16[320,2048]{1,0:T(8,128)(2,1)}) %all-gather.11.cloned.1.call-update) | async-done | bytes 1310736 | tf_op jit(solution)/shard_map/all_gather | solution.py:163
  66.9 2.2 multiply_convert_fusion.2
  69.8 1.6 fusion
  73.9 2.0 convolution_bitcast_fusion.7
  76.5 21.5 %reduce-scatter.3.cloned.1.call-done = bf16[320,512]{1,0:T(8,128)(2,1)} async-done(((bf16[320,2048]{1,0:T(8,128)(2,1)}), bf16[320,512]{1,0:T(8,128)(2,1)}) %reduce-scatter.3.cloned.1.call-update) | async-done | bytes 327696 | tf_op jit(solution)/shard_map/reduce_scatter | solution.py:189
  98.0 5.5 %all-to-all-start.2 = ((bf16[8,40,512]{2,1,0:T(8,128)(2,1)}), bf16[8,40,512]{2,1,0:T(8,128)(2,1)S(1)}, u32[]{:S(2)}, u32[]{:S(2)}) async-start(bf16[8,40,512]{2,1,0:T(8,128)(2,1)} %bitcast.227), calls=%async_computation.3 | async-start | bytes 655360 | tf_op jit(solution)/shard_map/all_to_all | solution.py:190
  105.0 1.3 bitcast_multiply_fusion.4
  106.3 21.9 %all-gather.2 = f32[8,1,16]{2,1,0:T(1,128)S(1)} all-gather(f32[1,1,16]{2,1,0:T(1,128)} %get-tuple-element.531), channel_id=1, replica_groups=mesh['sp'=8,'tp'=4] {'sp'}, dimensions={0}, use_global_device_ids=true | all-gather | bytes 576 | tf_op jit(solution)/shard_map/all_gather | solution.py:24
  129.7 7.0 %all_gather.32 = bf16[128,2048]{1,0:T(8,128)(2,1)} all-gather(bf16[128,512]{1,0:T(8,128)(2,1)S(1)} %fusion.4), channel_id=1, replica_groups=mesh['sp'=8,'tp'=4] {'tp'}, dimensions={1}, use_global_device_ids=true | all-gather | bytes 655360 | tf_op jit(solution)/shard_map/all_gather | solution.py:193
  136.7 12.8 %all-gather.15.cloned.1.call-done = f32[128,64,128]{2,1,0:T(8,128)} async-done(((f32[16,64,128]{2,1,0:T(8,128)}), f32[128,64,128]{2,1,0:T(8,128)}) %all-gather.15.cloned.1.call-update) | async-done | bytes 4194320 | tf_op jit(solution)/shard_map/all_gather | solution.py:24
  149.8 2.1 convolution_bitcast_fusion.6
  152.0 2.0 fusion.1
  155.2 66.9 %all-gather.13.cloned.1.call-done = bf16[2048,1024]{1,0:T(8,128)(2,1)} async-done(((bf16[256,1024]{1,0:T(8,128)(2,1)}), bf16[2048,1024]{1,0:T(8,128)(2,1)}) %all-gather.13.cloned.1.call-update) | async-done | bytes 4194320 | tf_op jit(solution)/shard_map/all_gather | solution.py:217
  222.2 4.3 fusion.68
  226.5 2.3 mul.373
  228.8 1.9 reduce_sum.232
  230.7 1.4 copy.225
  232.1 2.3 mul.379
  234.4 1.9 reduce_sum.233
  236.3 1.5 copy.228
  237.7 1.3 multiply_multiply_fusion
  239.0 1.4 copy.226
  242.3 1.4 copy.229
  247.5 3.1 convolution_add_fusion.2
  250.9 6.0 %fusion.39 = f32[2048,1024]{1,0:T(8,128)} fusion(bf16[128,2048]{1,0:T(8,128)(2,1)} %all_gather.32, f32[128,1024]{1,0:T(8,128)} %bitcast.211, f32[128,1024]{1,0:T(8,128)} %copy-done.3, bf16[128,1024]{1,0:T(8,128)(2,1)} %param.29), kind=kOutput, calls=%fused_computation.85 | convolution fusion | flops 537919488 | bytes 10223616 | tf_op jit(solution)/shard_map/dot_general | solution.py:209
  256.9 1.8 fusion.43
  258.7 2.1 convolution_bitcast_fusion.1
  260.8 2.1 convolution_bitcast_fusion.2
  262.9 2.1 convolution_bitcast_fusion
  265.7 1.4 copy.239
  267.1 2.6 bitcast_reduce_fusion.2
  269.7 1.3 fusion.25
  271.0 1.4 copy.240
  272.4 1.4 copy.241
  273.8 2.5 bitcast_reduce_fusion
  276.3 1.7 copy.237
  278.0 1.9 fusion.5
  279.9 1.7 copy.245
  281.6 3.2 convolution_add_fusion.3
  284.7 37.2 %all-gather.17.cloned.1.call-done = f32[128,64,128]{2,1,0:T(8,128)} async-done(((f32[16,64,128]{2,1,0:T(8,128)}), f32[128,64,128]{2,1,0:T(8,128)}) %all-gather.17.cloned.1.call-update) | async-done | bytes 4194320 | tf_op jit(solution)/shard_map/all_gather | solution.py:24
  322.0 13.6 %while.20 = (s32[]{:T(128)}, f32[16,64,128]{2,1,0:T(8,128)S(1)}, s32[]{:T(128)}, f32[8,16]{1,0:T(8,128)}, f32[8,16,64,128]{3,2,1,0:T(8,128)}, /*index=5*/s32[]{:T(128)}, s32[]{:T(128)}, s32[]{:T(128)}, s32[]{:T(128)}) while((s32[]{:T(128)}, f32[16,64,128]{2,1,0:T(8,128)S(1)}, s32[]{:T(128)}, f32[8,16]{1,0:T(8,128)}, ...), condition=%wide.region_13.14_spmd, body=%wide.region_12.13_spmd.sunk | while | flops 262150 | bytes 1573203 | solution.py:33
  336.6 1.3 bitcast_reduce_fusion.3
  343.6 1.3 fusion.7
  347.6 124.5 %reduce-scatter.5.cloned.1.call-done = f32[256,1024]{1,0:T(8,128)} async-done(((f32[2048,1024]{1,0:T(8,128)}), f32[256,1024]{1,0:T(8,128)}) %reduce-scatter.5.cloned.1.call-update) | async-done | bytes 1048592 | tf_op jit(solution)/shard_map/reduce_scatter | solution.py:208
  (188 shorter events, 42.6 us)
Async XLA Ops:
  8.0 39.1 %copy-start = (bf16[1,2048,256]{2,1,0:T(8,128)(2,1)S(1)}, bf16[1,2048,256]{2,1,0:T(8,128)(2,1)}, u32[]{:S(2)}) copy-start(bf16[1,2048,256]{2,1,0:T(8,128)(2,1)} %param.21) | copy-start | bytes 3145732
  8.0 22.4 %copy-start.45 = (f32[128,2]{0,1:T(2,128)S(1)}, f32[128,2]{0,1:T(2,128)}, u32[]{:S(2)}) copy-start(f32[128,2]{0,1:T(2,128)} %param.20) | copy-start | bytes 3076
  8.0 22.6 %copy-start.29 = (bf16[128,512]{1,0:T(8,128)(2,1)S(1)}, bf16[128,512]{1,0:T(8,128)(2,1)}, u32[]{:S(2)}) copy-start(bf16[128,512]{1,0:T(8,128)(2,1)} %param.18) | copy-start | bytes 393220
  8.0 39.1 %all-gather.9.cloned.1.call-start = ((), (), s32[]{:S(2)}) async-start(), calls=%async_computation.5 | async-start | bytes 1638400 | tf_op jit(solution)/shard_map/all_gather | solution.py:162
  11.1 33.5 %copy-start.41 = (s32[128]{0:T(128)}, s32[128]{0:T(128)S(1)}, u32[]{:S(2)}) copy-start(s32[128]{0:T(128)S(1)} %get-tuple-element.536) | copy-start | bytes 1540
  11.1 33.5 %copy-start.42 = (s32[128]{0:T(128)}, s32[128]{0:T(128)S(1)}, u32[]{:S(2)}) copy-start(s32[128]{0:T(128)S(1)} %get-tuple-element.537) | copy-start | bytes 1540
  30.4 36.5 %all-gather.11.cloned.1.call-start = ((), (), s32[]{:S(2)}) async-start(), calls=%async_computation.6 | async-start | bytes 1638400 | tf_op jit(solution)/shard_map/all_gather | solution.py:163
  44.7 4.4 copy-start.17
  44.7 53.3 %reduce-scatter.3.cloned.1.call-start = ((), (), s32[]{:S(2)}) async-start(), calls=%async_computation.7 | async-start | bytes 1638400 | tf_op jit(solution)/shard_map/reduce_scatter | solution.py:189
  47.1 1.9 copy-start.4
  49.1 17.8 %copy-start.30 = (f32[320,256]{1,0:T(8,128)}, f32[320,256]{1,0:T(8,128)S(1)}, u32[]{:S(2)}) copy-start(f32[320,256]{1,0:T(8,128)S(1)} %fusion.15) | copy-start | bytes 983044
  49.6 19.5 %copy-start.32 = (f32[320,256]{1,0:T(8,128)}, f32[320,256]{1,0:T(8,128)S(1)}, u32[]{:S(2)}) copy-start(f32[320,256]{1,0:T(8,128)S(1)} %fusion.18) | copy-start | bytes 983044
  69.1 0.7 copy-start.21
  71.4 1.6 copy-start.39
  71.4 2.2 copy-start.34
  71.5 78.0 %all-gather.15.cloned.1.call-start = ((), (), s32[]{:S(2)}) async-start(), calls=%async_computation.10 | async-start | bytes 4718592 | tf_op jit(solution)/shard_map/all_gather | solution.py:24
  72.4 55.8 %copy-start.15 = (f32[128,16]{1,0:T(8,128)}, f32[128,16]{1,0:T(8,128)S(1)}, u32[]{:S(2)}) copy-start(f32[128,16]{1,0:T(8,128)S(1)} %reduce_window_sum.53) | copy-start | bytes 24580
  73.0 2.8 copy-start.37
  75.9 27.7 %copy-start.40 = (bf16[128,256]{1,0:T(8,128)(2,1)S(1)}, bf16[128,256]{1,0:T(8,128)(2,1)}, u32[]{:S(2)}) copy-start(bf16[128,256]{1,0:T(8,128)(2,1)} %param.27) | copy-start | bytes 196612
  75.9 146.3 %all-gather.13.cloned.1.call-start = ((), (), s32[]{:S(2)}) async-start(), calls=%async_computation.9 | async-start | bytes 4718592 | tf_op jit(solution)/shard_map/all_gather | solution.py:217
  98.0 30.8 %all-to-all-start.2 = ((bf16[8,40,512]{2,1,0:T(8,128)(2,1)}), bf16[8,40,512]{2,1,0:T(8,128)(2,1)S(1)}, u32[]{:S(2)}, u32[]{:S(2)}) async-start(bf16[8,40,512]{2,1,0:T(8,128)(2,1)} %bitcast.227), calls=%async_computation.3 | async-start | bytes 655360 | tf_op jit(solution)/shard_map/all_to_all | solution.py:190
  103.5 218.4 %all-gather.17.cloned.1.call-start = ((), (), s32[]{:S(2)}) async-start(), calls=%async_computation.11 | async-start | bytes 4718592 | tf_op jit(solution)/shard_map/all_gather | solution.py:24
  103.8 32.9 %copy-start.25 = (bf16[128,2,128]{0,2,1:T(8,128)(2,1)}, bf16[128,2,128]{0,2,1:T(8,128)(2,1)S(1)}, u32[]{:S(2)}) copy-start(bf16[128,2,128]{0,2,1:T(8,128)(2,1)S(1)} %copy.234) | copy-start | bytes 196612
  104.9 44.6 %copy-start.13 = (f32[128,128,2]{1,0,2:T(8,128)}, f32[128,128,2]{1,0,2:T(8,128)S(1)}, u32[]{:S(2)}) copy-start(f32[128,128,2]{1,0,2:T(8,128)S(1)} %copy.214) | copy-start | bytes 393220
  105.0 23.8 %copy-start.35 = (pred[128,128]{1,0:T(8,128)(4,1)}, pred[128,128]{1,0:T(8,128)(4,1)S(1)}, u32[]{:S(2)}) copy-start(pred[128,128]{1,0:T(8,128)(4,1)S(1)} %iota_compare_fusion.2) | copy-start | bytes 49156
  149.7 2.3 copy-start.44
  149.8 4.2 copy-start.1
  149.8 2.2 copy-start.2
  152.0 2.0 copy-start.7
  155.2 89.8 %copy-start.3 = (f32[128,1024]{1,0:T(8,128)}, f32[128,1024]{1,0:T(8,128)S(1)}, u32[]{:S(2)}) copy-start(f32[128,1024]{1,0:T(8,128)S(1)} %copy.224) | copy-start | bytes 1572868
  243.8 1.3 copy-start.6
  243.8 1.3 copy-start.9
  243.8 1.3 copy-start.11
  250.6 221.5 %reduce-scatter.5.cloned.1.call-start = ((), (), s32[]{:S(2)}) async-start(), calls=%async_computation.8 | async-start | bytes 9437184 | tf_op jit(solution)/shard_map/reduce_scatter | solution.py:208
  256.9 1.8 copy-start.5
  256.9 1.8 copy-start.22
  258.7 2.1 copy-start.24
  260.8 2.1 copy-start.12
  260.8 2.1 copy-start.31
  260.8 2.1 copy-start.33
  262.9 2.1 copy-start.8
  267.1 2.6 copy-start.14
  267.1 2.6 copy-start.36
  335.6 1.0 copy-start.38
  337.9 0.8 copy-start.19
  338.1 1.5 copy-start.16
  338.1 1.5 copy-start.20
  339.6 6.1 %copy-start.10 = (f32[16,64,128]{2,1,0:T(8,128)S(1)}, f32[16,64,128]{2,1,0:T(8,128)}, u32[]{:S(2)}) copy-start(f32[16,64,128]{2,1,0:T(8,128)} %convolution_add_fusion.3) | copy-start | bytes 1572868
  (6 other events, 3.9 us)
Sparse Core Ops, SparseCore 0:
  30.5 16.5 all-gather.8
  48.7 18.1 all-gather.10
  71.6 26.3 reduce-scatter.2
Sparse Core Ops, SparseCore 1:
  76.0 73.4 all-gather.14
  151.5 70.7 all-gather.12
  250.7 71.1 all-gather.16
  326.1 145.9 reduce-scatter.4
where the time goes:
time: 481 us; the launch traced here: 479 us
  waiting for transfers between devices  283 us (59%)
  blocking collectives  60.6 us (13%)
  matrix products  51.6 us (11%)
  local copies, waits for them, and re-layouts  37.1 us (8%)
  other arithmetic  24.1 us (5%)
  between operations  16.1 us (3%)
  starting transfers between devices  6.02 us (1%)
    reduce_scatter x1, waiting for transfers between devices, local(): lax.psum_scatter(lax.dot_general(columns, normed_half, by_rows, preferred...  125 us
    all_gather x1, waiting for transfers between devices, local(): lax.all_gather(out_weight, 'sp', axis=0, tiled=True)  66.9 us
    all_gather x2, waiting for transfers between devices, entering(): gathered = jax.tree.map(lambda a: lax.all_gather(a, axis), part)  50 us
    all_gather x1, blocking collectives, entering(): gathered = jax.tree.map(lambda a: lax.all_gather(a, axis), part)  21.9 us
    reduce_scatter x1, waiting for transfers between devices, local(): lax.psum_scatter(stacked.astype(jnp.bfloat16), 'tp', scatter_dimension=1,...  21.5 us
    all_to_all x1, blocking collectives, local(): lax.all_to_all(sent_rows, 'sp', split_axis=0, concat_axis=0, tiled=True)  18.1 us
    all_gather x1, waiting for transfers between devices, local(): lax.all_gather(part_cot, 'tp', axis=1, tiled=True)  17.3 us
    all_to_all x1, blocking collectives, local(): lax.all_to_all(sent_cot, 'sp', split_axis=0, concat_axis=0, tiled=True)  13.7 us
  transfers between devices with their start and end apart: 8, of which 7 were waited for; matrix products, arithmetic and copies ran while one was open for 15% of the time, Pallas kernels for 0%

commit v1 on v0

v1 whole, which is shorter than its diff:
```python
from functools import partial, reduce

import jax
import jax.numpy as jnp
from jax import lax
from jax.experimental import pallas as pl
from jax.experimental.pallas import tpu as pltpu
from jax.sharding import PartitionSpec as P

D = 2048
HEAD_DIM = 64
NS = 128
TAIL = 16

epsilon = 1e-06
exact_mode = lax.Precision.HIGHEST
f32 = jnp.float32
bf16 = jnp.bfloat16
by_rows = (((0,), (0,)), ((), ()))
by_cols = (((1,), (1,)), ((), ()))


def dot(a, b, dims=(((1,), (0,)), ((), ()))):
    return lax.dot_general(a, b, dims, preferred_element_type=f32)


def exact(a, b, dims=(((1,), (0,)), ((), ()))):
    return lax.dot_general(a, b, dims, precision=exact_mode, preferred_element_type=f32)


def iota(shape, dim):
    return lax.broadcasted_iota(jnp.int32, shape, dim)


def lower(length):
    return iota((length, length), 0) >= iota((length, length), 1)


def spread(heads):
    shape = (heads, heads * HEAD_DIM)
    return (iota(shape, 1) // HEAD_DIM == iota(shape, 0)).astype(f32)


def cum_logs(log):
    return exact(lower(log.shape[0]).astype(f32), log)


def state_kernel(x_ref, b_ref, log_ref, sent_ref, own_ref):
    length, heads = log_ref.shape
    groups = b_ref.shape[1] // NS
    wide = x_ref.shape[1] // groups
    cum = cum_logs(log_ref[...])
    last = cum[length - 1 : length, :]
    to_end = exact(jnp.exp(last - cum), spread(heads))
    weighted = (x_ref[...].astype(f32) * to_end).astype(bf16)
    for g in range(groups):
        state = dot(weighted[:, g * wide : (g + 1) * wide], b_ref[:, g * NS : (g + 1) * NS], by_rows)
        own_ref[g * wide : (g + 1) * wide, :] = state
        sent_ref[g * wide : (g + 1) * wide, :] = state.astype(bf16)
    row = jnp.concatenate([last, jnp.zeros((1, NS - heads), f32)], axis=1)
    high = row.astype(bf16).astype(f32)
    middle = (row - high).astype(bf16).astype(f32)
    low = row - high - middle
    sent_ref[heads * HEAD_DIM :, :] = jnp.concatenate(
        [high, middle, low, jnp.zeros((TAIL - 3, NS), f32)], axis=0
    ).astype(bf16)


def combine(weights_ref, parts_ref, total_ref):
    count, heads = weights_ref.shape

    def one(source, _):
        for h in range(heads):
            rows = slice(h * HEAD_DIM, (h + 1) * HEAD_DIM)
            total_ref[rows, :] += weights_ref[source, h] * parts_ref[source, rows, :].astype(f32)
        return 0

    total_ref[...] = jnp.zeros_like(total_ref)
    lax.fori_loop(0, count, one, 0)


def decay_of(cum, cum_t, mask, h):
    spans = jnp.where(mask, cum[:, h : h + 1] - cum_t[h : h + 1, :], 0.0)
    return jnp.where(mask, jnp.exp(spans), 0.0)


def forward_kernel(
    weights_ref, parts_ref, x_ref, b_ref, c_ref, log_ref, z_ref, entry_ref, y_ref, half_ref
):
    length, heads = log_ref.shape
    groups = b_ref.shape[1] // NS
    wide = x_ref.shape[1] // groups
    per_group = heads // groups
    combine(weights_ref, parts_ref, entry_ref)
    log = log_ref[...]
    mask = lower(length)
    cum = cum_logs(log)
    cum_t = exact(log, mask.astype(f32), (((0,), (1,)), ((), ())))
    grown = exact(jnp.exp(cum), spread(heads))
    for g in range(groups):
        cols = slice(g * wide, (g + 1) * wide)
        c = c_ref[:, g * NS : (g + 1) * NS]
        scores = dot(c, b_ref[:, g * NS : (g + 1) * NS], by_cols)
        carried = dot(c, entry_ref[cols, :].astype(bf16), by_cols) * grown[:, cols]
        within = [
            dot(
                (scores * decay_of(cum, cum_t, mask, h)).astype(bf16),
                x_ref[:, h * HEAD_DIM : (h + 1) * HEAD_DIM],
            )
            for h in range(g * per_group, (g + 1) * per_group)
        ]
        y = carried + jnp.concatenate(within, axis=1)
        y_ref[:, cols] = y
        gated = y * jax.nn.silu(z_ref[:, cols].astype(f32))
        scale = lax.rsqrt(jnp.mean(gated * gated, axis=1, keepdims=True) + epsilon)
        half_ref[:, cols] = (gated * scale).astype(bf16)


def gate_kernel(dn_ref, y_ref, z_ref, c_ref, log_ref, dy_ref, dz_ref, sent_ref):
    length, heads = log_ref.shape
    groups = c_ref.shape[1] // NS
    wide = y_ref.shape[1] // groups
    grown = exact(jnp.exp(cum_logs(log_ref[...])), spread(heads))
    for g in range(groups):
        cols = slice(g * wide, (g + 1) * wide)
        y = y_ref[:, cols]
        z = z_ref[:, cols].astype(f32)
        dn = dn_ref[:, cols]
        sig = jax.nn.sigmoid(z)
        silu = z * sig
        gated = y * silu
        scale = lax.rsqrt(jnp.mean(gated * gated, axis=1, keepdims=True) + epsilon)
        normed = gated * scale
        d_gated = scale * (dn - normed * jnp.mean(dn * normed, axis=1, keepdims=True))
        dy = d_gated * silu
        dy_ref[:, cols] = dy
        dz_ref[:, cols] = (d_gated * y * sig * (1.0 + z * (1.0 - sig))).astype(bf16)
        sent_ref[cols, :] = dot(
            (dy * grown[:, cols]).astype(bf16), c_ref[:, g * NS : (g + 1) * NS], by_rows
        ).astype(bf16)


def within_kernel(
    dy_ref, y_ref, x_ref, b_ref, c_ref, log_ref, entry_ref, dx_ref, db_ref, dc_ref, dl_ref
):
    length, heads = log_ref.shape
    groups = b_ref.shape[1] // NS
    wide = x_ref.shape[1] // groups
    per_group = heads // groups
    log = log_ref[...]
    mask = lower(length)
    cum = cum_logs(log)
    cum_t = exact(log, mask.astype(f32), (((0,), (1,)), ((), ())))
    grown = exact(jnp.exp(cum), spread(heads))
    balance = jnp.zeros((length, heads), f32)
    for g in range(groups):
        cols = slice(g * wide, (g + 1) * wide)
        maps = slice(g * NS, (g + 1) * NS)
        b, c = b_ref[:, maps], c_ref[:, maps]
        scores = dot(c, b, by_cols)
        dy = dy_ref[:, cols]
        dy_half = dy.astype(bf16)
        x = x_ref[:, cols]
        d_scores = jnp.zeros((length, length), f32)
        dx = []
        for k in range(per_group):
            h = g * per_group + k
            part = slice(k * HEAD_DIM, (k + 1) * HEAD_DIM)
            decay = decay_of(cum, cum_t, mask, h)
            d_scores = d_scores + dot(dy_half[:, part], x[:, part], by_cols) * decay
            dx.append(dot((scores * decay).astype(bf16), dy_half[:, part], by_rows))
        dx = jnp.concatenate(dx, axis=1)
        dx_ref[:, cols] = dx
        d_half = d_scores.astype(bf16)
        entry = entry_ref[cols, :].astype(bf16)
        dc_ref[:, maps] = dot(d_half, b) + dot((dy * grown[:, cols]).astype(bf16), entry)
        db_ref[:, maps] = dot(d_half, c, by_rows)
        balance = balance + exact(
            dy * y_ref[:, cols] - x.astype(f32) * dx, spread(heads)[:, cols], by_cols
        )
    dl_ref[...] = balance


def finish_kernel(
    weights_ref, parts_ref, x_ref, b_ref, log_ref, entry_ref, own_ref, dx_ref, db_ref, dl_ref,
    step_ref, map_ref, grad_log_ref, later_ref
):
    length, heads = log_ref.shape
    groups = b_ref.shape[1] // NS
    wide = x_ref.shape[1] // groups
    combine(weights_ref, parts_ref, later_ref)
    cum = cum_logs(log_ref[...])
    last = cum[length - 1 : length, :]
    to_end = exact(jnp.exp(last - cum), spread(heads))
    balance = dl_ref[...]
    crossing = []
    for g in range(groups):
        cols = slice(g * wide, (g + 1) * wide)
        maps = slice(g * NS, (g + 1) * NS)
        later = later_ref[cols, :].astype(bf16)
        x = x_ref[:, cols].astype(f32)
        extra = dot(b_ref[:, maps], later, by_cols) * to_end[:, cols]
        step_ref[:, cols] = (dx_ref[:, cols] + extra).astype(bf16)
        map_ref[:, maps] = db_ref[:, maps] + dot((x * to_end[:, cols]).astype(bf16), later)
        balance = balance - exact(x * extra, spread(heads)[:, cols], by_cols)
    rows = (heads, HEAD_DIM, NS)
    own_sum = jnp.sum((later_ref[...] * own_ref[...]).reshape(rows), axis=1)
    entry_sum = jnp.sum((later_ref[...] * entry_ref[...]).reshape(rows), axis=1)
    ones = jnp.ones((1, NS), f32)
    through = exact(ones, own_sum, by_cols) + jnp.exp(last) * exact(ones, entry_sum, by_cols)
    grad_log_ref[...] = exact(lower(length).astype(f32), balance, by_rows) + through


def call(kernel, outs, *args, scalars=0, scratch=()):
    vmem = pl.BlockSpec(memory_space=pltpu.VMEM)
    smem = pl.BlockSpec(memory_space=pltpu.SMEM)
    return pl.pallas_call(
        kernel,
        out_shape=[jax.ShapeDtypeStruct(*o) for o in outs],
        in_specs=[smem] * scalars + [vmem] * (len(args) - scalars),
        out_specs=[vmem] * len(outs),
        scratch_shapes=list(scratch),
        compiler_params=pltpu.CompilerParams(vmem_limit_bytes=56 * 1024 * 1024),
    )(*args)


def expert_backward(row_block, cot_block, gate_mat, up_mat, down_mat):
    gate_pre = jnp.dot(row_block, gate_mat, preferred_element_type=jnp.float32)
    up_pre = jnp.dot(row_block, up_mat, preferred_element_type=jnp.float32)
    gate_sigmoid = jax.nn.sigmoid(gate_pre)
    hidden = (gate_pre * gate_sigmoid * up_pre).astype(jnp.bfloat16)
    d_act = lax.dot_general(cot_block, down_mat, by_cols, preferred_element_type=jnp.float32)
    d_gate = (d_act * up_pre * gate_sigmoid * (1.0 + gate_pre * (1.0 - gate_sigmoid))).astype(
        jnp.bfloat16
    )
    d_up = (d_act * gate_pre * gate_sigmoid).astype(jnp.bfloat16)
    grad_down = lax.dot_general(hidden, cot_block, by_rows, preferred_element_type=jnp.float32)
    grad_gate = lax.dot_general(row_block, d_gate, by_rows, preferred_element_type=jnp.float32)
    grad_up = lax.dot_general(row_block, d_up, by_rows, preferred_element_type=jnp.float32)
    input_part = lax.dot_general(d_gate, gate_mat, by_cols, preferred_element_type=jnp.float32)
    input_part = input_part + lax.dot_general(
        d_up, up_mat, by_cols, preferred_element_type=jnp.float32
    )
    return (grad_gate, grad_up, grad_down, input_part)


def local(
    hidden_rows,
    out_cot,
    routes,
    route_weight,
    gate_w,
    up_w,
    down_w,
    out_weight,
    step_inputs,
    input_map,
    output_map,
    log_decay,
    gate_z,
):
    wide = step_inputs.shape
    heads = log_decay.shape[1]
    states = (heads * HEAD_DIM, NS)
    place_sp = lax.axis_index("sp")
    sent_state, own_state = call(
        state_kernel,
        [((states[0] + TAIL, NS), bf16), (states, f32)],
        step_inputs, input_map, log_decay,
    )
    state_parts = lax.all_gather(sent_state, "sp")
    totals = jnp.sum(state_parts[:, states[0] : states[0] + 3, :heads].astype(f32), axis=1)
    sources = jnp.arange(lax.axis_size("sp"))
    before = ((sources[None, :] > sources[:, None]) & (sources[None, :] < place_sp)).astype(f32)
    after = ((sources[None, :] < sources[:, None]) & (sources[None, :] > place_sp)).astype(f32)
    entry_weights = jnp.where(
        (sources < place_sp)[:, None], jnp.exp(exact(before, totals)), 0.0
    )
    later_weights = jnp.where(
        (sources > place_sp)[:, None], jnp.exp(exact(after, totals)), 0.0
    )
    entry_state, y, normed_half = call(
        forward_kernel,
        [(states, f32), (wide, f32), (wide, bf16)],
        entry_weights, state_parts, step_inputs, input_map, output_map, log_decay, gate_z,
        scalars=1,
    )
    all_weight = lax.all_gather(out_weight, "sp", axis=0, tiled=True)
    all_half = lax.all_gather(normed_half, "sp", axis=0, tiled=True)
    tok_rows, top_count = routes.shape
    local_experts = gate_w.shape[0]
    sp_devices = lax.axis_size("sp")
    total_experts = local_experts * sp_devices
    capacity = 5 * tok_rows * top_count // (4 * total_experts)
    flat_routes = routes.reshape(-1)
    expert_hits = (
        flat_routes[:, None] == jnp.arange(total_experts, dtype=jnp.int32)[None, :]
    ).astype(jnp.int32)
    slot_rank = jnp.sum((jnp.cumsum(expert_hits, axis=0) - expert_hits) * expert_hits, axis=1)
    target = (flat_routes * capacity + slot_rank).reshape(tok_rows, top_count)
    slot_ids = jnp.arange(total_experts * capacity, dtype=jnp.int32)[:, None]
    matches = [slot_ids == target[:, column][None, :] for column in range(top_count)]
    placing = reduce(jnp.logical_or, matches).astype(jnp.bfloat16)
    slot_weight = reduce(
        jnp.add,
        [
            jnp.sum(jnp.where(matches[column], route_weight[:, column][None, :], 0.0), axis=1)
            for column in range(top_count)
        ],
    )

    def place(source_rows):
        return jnp.dot(placing, source_rows, preferred_element_type=jnp.float32)

    sent_rows = place(hidden_rows).astype(jnp.bfloat16)
    sent_cot = (place(out_cot) * slot_weight[:, None]).astype(jnp.bfloat16)
    part_rows, part_cot = (
        lax.all_to_all(sent_rows, "sp", split_axis=0, concat_axis=0, tiled=True),
        lax.all_to_all(sent_cot, "sp", split_axis=0, concat_axis=0, tiled=True),
    )
    got_rows, got_cot = (
        lax.all_gather(part_rows, "tp", axis=1, tiled=True),
        lax.all_gather(part_cot, "tp", axis=1, tiled=True),
    )
    buffer_rows = sp_devices * capacity
    arranged_rows = (
        got_rows.reshape(sp_devices, local_experts, capacity, D)
        .transpose(1, 0, 2, 3)
        .reshape(local_experts, buffer_rows, D)
    )
    arranged_cot = (
        got_cot.reshape(sp_devices, local_experts, capacity, D)
        .transpose(1, 0, 2, 3)
        .reshape(local_experts, buffer_rows, D)
    )
    grad_gate, grad_up, grad_down, input_part = expert_backward(
        arranged_rows[0], arranged_cot[0], gate_w[0], up_w[0], down_w[0]
    )
    grads_gate = [grad_gate]
    grads_up = [grad_up]
    grads_down = [grad_down]
    partials = [input_part]
    stacked = (
        jnp.stack(partials)
        .reshape(local_experts, sp_devices, capacity, D)
        .transpose(1, 0, 2, 3)
        .reshape(-1, D)
    )
    tp_devices = lax.axis_size("tp")
    pieces = stacked.astype(bf16).reshape(-1, tp_devices, D // tp_devices).transpose(1, 0, 2)
    pieces = lax.all_to_all(pieces, "tp", split_axis=0, concat_axis=0, tiled=True)
    summed = jnp.sum(pieces.astype(f32), axis=0).astype(bf16)
    returned = lax.all_to_all(summed, "sp", split_axis=0, concat_axis=0, tiled=True)
    routed = lax.dot_general(placing, returned, by_rows, preferred_element_type=jnp.float32)
    mid_part = (out_cot.astype(jnp.float32) + routed).astype(jnp.bfloat16)
    mid_grad = lax.all_gather(mid_part, "tp", axis=1, tiled=True)
    mid_cols = lax.all_to_all(mid_grad, "sp", split_axis=1, concat_axis=0, tiled=True)
    d_normed = dot(mid_grad, all_weight)
    dy, grad_gate_z, sent_grad = call(
        gate_kernel,
        [(wide, f32), (wide, bf16), (states, bf16)],
        d_normed, y, gate_z, output_map, log_decay,
    )
    later_parts = lax.all_gather(sent_grad, "sp")
    dx, db, dc, dl = call(
        within_kernel,
        [(wide, f32), (input_map.shape, f32), (output_map.shape, f32), (log_decay.shape, f32)],
        dy, y, step_inputs, input_map, output_map, log_decay, entry_state,
    )
    grad_out_weight = dot(mid_cols, all_half, by_rows)
    grad_step, grad_in_map, grad_log = call(
        finish_kernel,
        [(wide, bf16), (input_map.shape, f32), (log_decay.shape, f32)],
        later_weights, later_parts, step_inputs, input_map, log_decay, entry_state, own_state,
        dx, db, dl,
        scalars=1,
        scratch=[pltpu.VMEM(states, f32)],
    )
    return (
        jnp.stack(grads_gate),
        jnp.stack(grads_up),
        jnp.stack(grads_down),
        grad_out_weight,
        grad_step,
        grad_gate_z,
        grad_in_map,
        dc,
        grad_log,
    )


def solution(mesh):
    placed = (
        P("sp", "tp"),
        P("sp", "tp"),
        P("sp", None),
        P("sp", None),
        P("sp", None, "tp"),
        P("sp", None, "tp"),
        P("sp", "tp", None),
        P("sp", "tp"),
        P("sp", "tp"),
        P("sp", "tp"),
        P("sp", "tp"),
        P("sp", "tp"),
        P("sp", "tp"),
    )
    return jax.shard_map(
        local,
        mesh=mesh,
        in_specs=placed,
        out_specs=(
            P("sp", None, "tp"),
            P("sp", None, "tp"),
            P("sp", "tp", None),
            P("sp", "tp"),
            P("sp", "tp"),
            P("sp", "tp"),
            P("sp", "tp"),
            P("sp", "tp"),
            P("sp", "tp"),
        ),
        check_vma=False,
    )
```

time: 481 us -> 308 us (0.64)
  waiting for transfers between devices: 283 us -> 139 us
  blocking collectives: 60.6 us -> 95.7 us
  local copies, waits for them, and re-layouts: 37.1 us -> 5.64 us
  matrix products: 51.6 us -> 23.6 us
  Pallas kernels: 0 us -> 20.9 us
  other arithmetic: 24.1 us -> 3.98 us
    reduce_scatter x2 -> x0, waiting for transfers between devices: 146 us -> none  [the longest x1 125 us: local(): lax.psum_scatter(lax.dot_general(columns, normed_half, by_rows, preferred...]
    all_to_all x0 -> x2, blocking collectives: none -> 42.6 us  [the longest x1 22.2 us: local(): lax.all_to_all(summed, 'sp', split_axis=0, concat_axis=0, tiled=True)]
    dot_general x16 -> x4, matrix products: 36.3 us -> 8.44 us  [the longest x2 6.99 us: dot(): return lax.dot_general(a, b, dims, preferred_element_type=f32)]
    all_gather x1 -> x0, blocking collectives: 21.9 us -> none  [entering(): gathered = jax.tree.map(lambda a: lax.all_gather(a, axis), part)]
    pallas_call x0 -> x5, Pallas kernels: none -> 20.9 us  [call(): pl.pallas_call(kernel, out_shape=[jax.ShapeDtypeStruct(*o) for o in outs]...]
    all_gather x3 -> x4, waiting for transfers between devices: 117 us -> 101 us  [the longest x1 46.3 us: local(): later_parts = lax.all_gather(sent_grad, 'sp')]
    mul x11 -> x0, local copies, waits for them, and re-layouts: 11.7 us -> none  [the longest x7 4.87 us: compose_steps(): earlier[1] * later[0][:, None, None] + later[1]]
    all_gather x1, waiting for transfers between devices: 2.42 us -> 12.7 us  [local(): lax.all_gather(part_rows, 'tp', axis=1, tiled=True)]
  transfers between devices with their start and end apart: 8 -> 7, of which waited for: 7 -> 7; matrix products, arithmetic and copies ran while one was open for 15% -> 10% of each run, Pallas kernels for 0% -> 4%
where the time goes in v1:
time: 308 us; the launch traced here: 307 us
  waiting for transfers between devices  139 us (45%)
  blocking collectives  95.7 us (31%)
  matrix products  23.6 us (8%)
  Pallas kernels  20.9 us (7%)
  between operations  14.3 us (5%)
  local copies, waits for them, and re-layouts  5.64 us (2%)
  other arithmetic  3.98 us (1%)
  starting transfers between devices  3.92 us (1%)
    all_gather x1, waiting for transfers between devices, local(): later_parts = lax.all_gather(sent_grad, 'sp')  46.3 us
    all_to_all x1, blocking collectives, local(): lax.all_to_all(sent_rows, 'sp', split_axis=0, concat_axis=0, tiled=True)  25.6 us
    all_gather x1, waiting for transfers between devices, local(): all_half = lax.all_gather(normed_half, 'sp', axis=0, tiled=True)  24.6 us
    all_to_all x1, blocking collectives, local(): lax.all_to_all(summed, 'sp', split_axis=0, concat_axis=0, tiled=True)  22.2 us
    all_gather x1, waiting for transfers between devices, local(): all_weight = lax.all_gather(out_weight, 'sp', axis=0, tiled=True)  21.6 us
    all_to_all x1, blocking collectives, local(): lax.all_to_all(sent_cot, 'sp', split_axis=0, concat_axis=0, tiled=True)  21 us
    pallas_call x5, Pallas kernels, call(): pl.pallas_call(kernel, out_shape=[jax.ShapeDtypeStruct(*o) for o in outs]...  20.9 us
    all_to_all x1, blocking collectives, local(): lax.all_to_all(pieces, 'tp', split_axis=0, concat_axis=0, tiled=True)  20.4 us
  transfers between devices with their start and end apart: 7, of which 7 were waited for; matrix products, arithmetic and copies ran while one was open for 10% of the time, Pallas kernels for 4%

profile of v1, /device:TPU:0, one launch (start us, length us, event | category | flops | bytes accessed | tf_op | source)
XLA Modules:
  0.0 307.1 jit_solution(10651969010922189704)
XLA Ops:
  7.3 1.5 copy.79.log_ref
  8.8 2.9 shard_map.196
  11.7 0.8 copy.74
  12.5 0.1 eq.60
  12.6 0.1 eq.56
  12.8 0.6 reduce-window.6
  13.4 0.2 slice_reduce_fusion
  13.7 0.1 reduce_sum.51
  13.9 0.7 multiply_add_fusion
  14.6 1.1 convolution_convert_fusion
  15.8 25.6 %all_to_all.60 = bf16[8,40,512]{2,1,0:T(8,128)(2,1)} all-to-all(bf16[8,40,512]{2,1,0:T(8,128)(2,1)S(1)} %bitcast.89), channel_id=1, replica_groups=mesh['sp'=8,'tp'=4] {'sp'}, dimensions={0} | all-to-all | bytes 655360 | tf_op jit(solution)/shard_map/all_to_all | solution.py:318
  41.5 0.2 select_reduce_fusion
  41.7 0.2 fusion.1
  41.9 21.0 %all_to_all.61 = bf16[8,40,512]{2,1,0:T(8,128)(2,1)} all-to-all(bf16[8,40,512]{2,1,0:T(8,128)(2,1)S(1)} %bitcast.88), channel_id=1, replica_groups=mesh['sp'=8,'tp'=4] {'sp'}, dimensions={0} | all-to-all | bytes 655360 | tf_op jit(solution)/shard_map/all_to_all | solution.py:319
  63.0 0.5 all-gather.15.cloned.1.call-update
  63.6 8.9 %all-gather.17.cloned.1.call-done = bf16[8320,128]{1,0:T(8,128)(2,1)} async-done(((bf16[1040,128]{1,0:T(8,128)(2,1)}), bf16[8320,128]{1,0:T(8,128)(2,1)}) %all-gather.17.cloned.1.call-update) | async-done | bytes 2129936 | tf_op jit(solution)/shard_map/all_gather | solution.py:271
  72.5 0.7 convert_reduce_fusion
  73.2 0.7 fusion.3.weights_ref
  74.0 4.6 %shard_map.197 = (f32[1024,128]{1,0:T(8,128)}, f32[128,1024]{1,0:T(8,128)}, bf16[128,1024]{1,0:T(8,128)(2,1)}) custom-call(f32[8,16]{1,0:T(8,128)} %fusion.3.weights_ref, bf16[8,1040,128]{2,1,0:T(8,128)(2,1)} %bitcast.82, bf16[128,1024]{1,0:T(8,128)(2,1)} %x_ref.7, bf16[128,256]{1,0:T(8,128)(2,1)} %b_ref.7, bf16[128,256]{1,0:T(8,128)(2,1)} %c_ref.5, ...), custom_call_target="tpu_custom_call" | custom-call | tf_op jit(solution)/shard_map/pallas_call | solution.py:217
  78.6 12.7 %all-gather.9.cloned.1.call-done = bf16[320,2048]{1,0:T(8,128)(2,1)} async-done(((bf16[320,512]{1,0:T(8,128)(2,1)}), bf16[320,2048]{1,0:T(8,128)(2,1)}) %all-gather.9.cloned.1.call-update) | async-done | bytes 1310736 | tf_op jit(solution)/shard_map/all_gather | solution.py:322
  91.3 2.7 fusion.10
  94.0 1.2 fusion.7
  95.2 15.9 %all-gather.11.cloned.1.call-done = bf16[320,2048]{1,0:T(8,128)(2,1)} async-done(((bf16[320,512]{1,0:T(8,128)(2,1)}), bf16[320,2048]{1,0:T(8,128)(2,1)}) %all-gather.11.cloned.1.call-update) | async-done | bytes 1310736 | tf_op jit(solution)/shard_map/all_gather | solution.py:323
  111.1 2.3 multiply_convert_fusion.1
  113.5 0.5 fusion.5
  114.2 0.5 fusion
  114.7 0.1 copy.89
  114.8 20.4 %all_to_all.62 = bf16[4,320,512]{2,1,0:T(8,128)(2,1)} all-to-all(bf16[4,320,512]{2,1,0:T(8,128)(2,1)S(1)} %bitcast.79), channel_id=1, replica_groups=mesh['sp'=8,'tp'=4] {'tp'}, dimensions={0} | all-to-all | bytes 2621440 | tf_op jit(solution)/shard_map/all_to_all | solution.py:351
  135.2 1.6 reduce_sum.54
  136.9 22.2 %all_to_all.63 = bf16[8,40,512]{2,1,0:T(8,128)(2,1)S(1)} all-to-all(bf16[8,40,512]{2,1,0:T(8,128)(2,1)S(1)} %bitcast.90), channel_id=1, replica_groups=mesh['sp'=8,'tp'=4] {'sp'}, dimensions={0} | all-to-all | bytes 655360 | tf_op jit(solution)/shard_map/all_to_all | solution.py:353
  159.0 0.3 fusion.2
  159.3 6.5 %all_gather.29 = bf16[128,2048]{1,0:T(8,128)(2,1)S(1)} all-gather(bf16[128,512]{1,0:T(8,128)(2,1)S(1)} %fusion.2), channel_id=1, replica_groups=mesh['sp'=8,'tp'=4] {'tp'}, dimensions={1}, use_global_device_ids=true | all-gather | bytes 655360 | tf_op jit(solution)/shard_map/all_gather | solution.py:356
  165.8 21.6 %all-gather.15.cloned.1.call-done = bf16[2048,1024]{1,0:T(8,128)(2,1)} async-done(((bf16[256,1024]{1,0:T(8,128)(2,1)}), bf16[2048,1024]{1,0:T(8,128)(2,1)}) %all-gather.15.cloned.1.call-update) | async-done | bytes 4194320 | tf_op jit(solution)/shard_map/all_gather | solution.py:288
  187.5 3.7 %fusion.36.dn_ref = f32[128,1024]{1,0:T(8,128)} fusion(bf16[128,2048]{1,0:T(8,128)(2,1)S(1)} %all_gather.29, bf16[2048,1024]{1,0:T(8,128)(2,1)} %all-gather.15.cloned.1.call-done), kind=kOutput, calls=%fused_computation.64 | convolution fusion | flops 536870912 | bytes 5242880 | tf_op jit(solution)/shard_map/dot_general | solution.py:24
  191.2 3.1 %shard_map.198 = (f32[128,1024]{1,0:T(8,128)}, bf16[128,1024]{1,0:T(8,128)(2,1)}, bf16[1024,128]{1,0:T(8,128)(2,1)}) custom-call(f32[128,1024]{1,0:T(8,128)} %fusion.36.dn_ref, f32[128,1024]{1,0:T(8,128)} %get-tuple-element.26.y_ref, bf16[128,1024]{1,0:T(8,128)(2,1)} %z_ref.3, bf16[128,256]{1,0:T(8,128)(2,1)} %c_ref.5, f32[128,16]{1,0:T(8,128)} %copy.79.log_ref), custom_call_target="tpu_custom_call" | custom-call | tf_op jit(solution)/shard_map/pallas_call | solution.py:217
  194.3 0.8 copy.90
  195.1 3.7 %all-to-all-start.4 = ((bf16[128,8,256]{2,0,1:T(8,128)(2,1)}), bf16[128,8,256]{2,0,1:T(8,128)(2,1)S(1)}, u32[]{:S(2)}, u32[]{:S(2)}) async-start(bf16[128,8,256]{2,0,1:T(8,128)(2,1)} %bitcast.77), calls=%async_computation.4 | async-start | bytes 1048576 | tf_op jit(solution)/shard_map/all_to_all | solution.py:357
  198.8 2.1 convolution_bitcast_fusion.1
  200.9 2.1 convolution_bitcast_fusion.2
  203.0 2.1 convolution_bitcast_fusion
  205.1 0.7 fusion.4.weights_ref
  205.8 5.3 %shard_map.199 = (f32[128,1024]{1,0:T(8,128)}, f32[128,256]{1,0:T(8,128)}, f32[128,256]{1,0:T(8,128)}, f32[128,16]{1,0:T(8,128)}) custom-call(f32[128,1024]{1,0:T(8,128)} %get-tuple-element.30.dy_ref, f32[128,1024]{1,0:T(8,128)} %get-tuple-element.26.y_ref, bf16[128,1024]{1,0:T(8,128)(2,1)} %x_ref.7, bf16[128,256]{1,0:T(8,128)(2,1)} %b_ref.7, ...), custom_call_target="tpu_custom_call" | custom-call | tf_op jit(solution)/shard_map/pallas_call | solution.py:217
  211.1 8.3 %all-to-all-done.4 = bf16[128,8,256]{2,0,1:T(8,128)(2,1)S(1)} async-done(((bf16[128,8,256]{2,0,1:T(8,128)(2,1)}), bf16[128,8,256]{2,0,1:T(8,128)(2,1)S(1)}, u32[]{:S(2)}, u32[]{:S(2)}) %all-to-all-start.4) | async-done | bytes 524320 | tf_op jit(solution)/shard_map/all_to_all | solution.py:357
  219.4 24.6 %all-gather.13.cloned.1.call-done = bf16[1024,1024]{1,0:T(8,128)(2,1)} async-done(((bf16[128,1024]{1,0:T(8,128)(2,1)}), bf16[1024,1024]{1,0:T(8,128)(2,1)}) %all-gather.13.cloned.1.call-update) | async-done | bytes 2097168 | tf_op jit(solution)/shard_map/all_gather | solution.py:289
  244.1 3.3 %fusion.35 = f32[256,1024]{1,0:T(8,128)} fusion(bf16[1024,256]{1,0:T(8,128)(2,1)S(1)} %bitcast.84, bf16[1024,1024]{1,0:T(8,128)(2,1)} %all-gather.13.cloned.1.call-done), kind=kOutput, calls=%fused_computation.63 | convolution fusion | flops 536870912 | bytes 3670016 | tf_op jit(solution)/shard_map/dot_general | solution.py:24
  247.4 46.3 %all-gather.19.cloned.1.call-done = bf16[8192,128]{1,0:T(8,128)(2,1)} async-done(((bf16[1024,128]{1,0:T(8,128)(2,1)}), bf16[8192,128]{1,0:T(8,128)(2,1)}) %all-gather.19.cloned.1.call-update) | async-done | bytes 2097168 | tf_op jit(solution)/shard_map/all_gather | solution.py:364
  293.7 5.1 %shard_map.200 = (bf16[128,1024]{1,0:T(8,128)(2,1)}, f32[128,256]{1,0:T(8,128)}, f32[128,16]{1,0:T(8,128)}) custom-call(f32[8,16]{1,0:T(8,128)} %fusion.4.weights_ref, bf16[8,1024,128]{2,1,0:T(8,128)(2,1)} %bitcast.83, bf16[128,1024]{1,0:T(8,128)(2,1)} %x_ref.7, bf16[128,256]{1,0:T(8,128)(2,1)} %b_ref.7, f32[128,16]{1,0:T(8,128)} %copy.79.log_ref, ...), custom_call_target="tpu_custom_call" | custom-call | tf_op jit(solution)/shard_map/pallas_call | solution.py:217
  298.8 1.5 copy.84
  (45 shorter events, 0.8 us)
Async XLA Ops:
  7.2 86.8 %copy-start = (bf16[1,2048,256]{2,1,0:T(8,128)(2,1)S(1)}, bf16[1,2048,256]{2,1,0:T(8,128)(2,1)}, u32[]{:S(2)}) copy-start(bf16[1,2048,256]{2,1,0:T(8,128)(2,1)} %param.17) | copy-start | bytes 3145732
  7.2 34.3 %copy-start.11 = (f32[128,2]{0,1:T(2,128)S(1)}, f32[128,2]{0,1:T(2,128)}, u32[]{:S(2)}) copy-start(f32[128,2]{0,1:T(2,128)} %param.16) | copy-start | bytes 3076
  7.2 34.5 %copy-start.8 = (bf16[128,512]{1,0:T(8,128)(2,1)S(1)}, bf16[128,512]{1,0:T(8,128)(2,1)}, u32[]{:S(2)}) copy-start(bf16[128,512]{1,0:T(8,128)(2,1)} %param.14) | copy-start | bytes 393220
  7.2 65.3 %all-gather.17.cloned.1.call-start = ((), (), s32[]{:S(2)}) async-start(), calls=%async_computation.9 | async-start | bytes 2396160 | tf_op jit(solution)/shard_map/all_gather | solution.py:271
  11.6 79.7 %all-gather.9.cloned.1.call-start = ((), (), s32[]{:S(2)}) async-start(), calls=%async_computation.5 | async-start | bytes 1638400 | tf_op jit(solution)/shard_map/all_gather | solution.py:322
  41.4 69.7 %all-gather.11.cloned.1.call-start = ((), (), s32[]{:S(2)}) async-start(), calls=%async_computation.6 | async-start | bytes 1638400 | tf_op jit(solution)/shard_map/all_gather | solution.py:323
  63.0 124.5 %all-gather.15.cloned.1.call-start = ((), (), s32[]{:S(2)}) async-start(), calls=%async_computation.8 | async-start | bytes 4718592 | tf_op jit(solution)/shard_map/all_gather | solution.py:288
  63.6 180.5 %all-gather.13.cloned.1.call-start = ((), (), s32[]{:S(2)}) async-start(), calls=%async_computation.7 | async-start | bytes 2359296 | tf_op jit(solution)/shard_map/all_gather | solution.py:289
  74.0 17.4 %copy-start.3 = (bf16[1,2048,256]{2,1,0:T(8,128)(2,1)S(1)}, bf16[1,2048,256]{2,1,0:T(8,128)(2,1)}, u32[]{:S(2)}) copy-start(bf16[1,2048,256]{2,1,0:T(8,128)(2,1)} %param.18) | copy-start | bytes 3145732
  78.6 215.1 %all-gather.19.cloned.1.call-start = ((), (), s32[]{:S(2)}) async-start(), calls=%async_computation.10 | async-start | bytes 2359296 | tf_op jit(solution)/shard_map/all_gather | solution.py:364
  91.3 2.7 copy-start.1
  113.4 0.7 copy-start.6
  113.4 0.7 copy-start.4
  194.2 4.6 %copy-start.5 = (bf16[320,256]{1,0:T(8,128)(2,1)S(1)}, bf16[320,256]{1,0:T(8,128)(2,1)}, u32[]{:S(2)}) copy-start(bf16[320,256]{1,0:T(8,128)(2,1)} %copy-done.4) | copy-start | bytes 491524
  195.1 24.3 %all-to-all-start.4 = ((bf16[128,8,256]{2,0,1:T(8,128)(2,1)}), bf16[128,8,256]{2,0,1:T(8,128)(2,1)S(1)}, u32[]{:S(2)}, u32[]{:S(2)}) async-start(bf16[128,8,256]{2,0,1:T(8,128)(2,1)} %bitcast.77), calls=%async_computation.4 | async-start | bytes 1048576 | tf_op jit(solution)/shard_map/all_to_all | solution.py:357
  198.8 2.1 copy-start.7
  200.9 2.1 copy-start.2
  200.9 2.1 copy-start.9
  200.9 2.1 copy-start.10
Sparse Core Ops, SparseCore 0:
  11.8 60.6 all-gather.16
  74.1 17.2 all-gather.8
  92.9 18.1 all-gather.10
  113.1 74.3 all-gather.14
  190.0 54.0 all-gather.12
  246.1 47.6 all-gather.18
